TPU v7x, 32 devices: a whole 2x2x4 slice. The times are simulated.
32 devices in a mesh: grp: 2 (over y), dp: 2 (over x), kv: 4 (over z), tp: 2 (over core).
Axes of the slice: x: 2, y: 2, z: 4, core: 2. Of those that a mesh axis runs over, the one named last changes fastest.
Arguments:
- tokens: bfloat16 [256, 4, 4096], P(('grp', 'dp'), None, ('kv', 'tp')), parts along dimension 0, may hold values from -160 to 160
- norm_gain: float32 [4096], replicated, may hold values from 0.1 to 1.9
- w_query: bfloat16 [4096, 16, 64], P(None, 'kv'), may hold values from -0.09375 to 0.09375
- w_key: bfloat16 [4096, 16, 64], P(None, 'kv'), may hold values from -0.09375 to 0.09375
- w_value: bfloat16 [4096, 16, 128], P(None, 'kv', 'tp'), may hold values from -0.09375 to 0.09375
- w_outgate: bfloat16 [4096, 16, 128], P(None, 'kv', 'tp'), may hold values from -0.09375 to 0.09375
- w_input: bfloat16 [4096, 16], replicated, may hold values from -0.09375 to 0.09375
- w_forget: bfloat16 [4096, 16], replicated, may hold values from -0.09375 to 0.09375
- forget_bias: float32 [16], replicated, may hold values from -1 to 4
- head_gain: float32 [16, 128], replicated, may hold values from 0.1 to 1.9
- w_out: bfloat16 [16, 128, 4096], P('kv', 'tp'), may hold values from -0.125 to 0.125
- memory: float32 [256, 16, 128, 64], P(('grp', 'dp'), 'kv', 'tp'), parts along dimension 0, may hold values from -12 to 12
- normalizer: float32 [256, 16, 64], P(('grp', 'dp'), 'kv'), parts along dimension 0, may hold values from -12 to 12
- stabilizer: float32 [256, 16], P(('grp', 'dp'), 'kv'), parts along dimension 0, may hold values from -1 to 1
- prev_keys: bfloat16 [256, 4, 16, 64], P(('grp', 'dp'), None, 'kv'), parts along dimension 0, may hold values from -6 to 6
- prev_values: bfloat16 [256, 4, 16, 128], P(('grp', 'dp'), None, 'kv', 'tp'), parts along dimension 0, may hold values from -6 to 6
- prev_input: float32 [256, 4, 16], P(('grp', 'dp'), None, 'kv'), parts along dimension 0, may hold values from -4 to 4
- prev_forget: float32 [256, 4, 16], P(('grp', 'dp'), None, 'kv'), parts along dimension 0, may hold values from -2 to -0.02
- accepted: int32 [256], P(('grp', 'dp')), parts along dimension 0, may hold values from 0 to 4
Outputs:
- mixed: bfloat16 [256, 4, 4096], P(('grp', 'dp'), None, ('kv', 'tp')), parts along dimension 0
- new_memory: float32 [256, 16, 128, 64], P(('grp', 'dp'), 'kv', 'tp'), parts along dimension 0
- new_normalizer: float32 [256, 16, 64], P(('grp', 'dp'), 'kv'), parts along dimension 0
- new_stabilizer: float32 [256, 16], P(('grp', 'dp'), 'kv'), parts along dimension 0
- new_keys: bfloat16 [256, 4, 16, 64], P(('grp', 'dp'), None, 'kv'), parts along dimension 0
- new_values: bfloat16 [256, 4, 16, 128], P(('grp', 'dp'), None, 'kv', 'tp'), parts along dimension 0
- new_input: float32 [256, 4, 16], P(('grp', 'dp'), None, 'kv'), parts along dimension 0
- new_forget: float32 [256, 4, 16], P(('grp', 'dp'), None, 'kv'), parts along dimension 0
There are 2 independent parts, one for each index of `grp`. A program takes and returns all parts, laid end to end along the dimension named above; an argument that names none is the same for every part. Nothing has to cross between parts.
All inputs are finite; a program needn't handle non-finite values.
Results may differ from a plain program's by a relative error of at most 0.038.
Values may be sent and summed in bfloat16 or wider, within the bound.
A program may use at most 128 MiB of HBM per device.

v0:
```python
import jax
import jax.numpy as jnp
from jax import lax
from jax.sharding import PartitionSpec as P

EPS = 1e-06
FAR_NEGATIVE = -1e30
HIGHEST_PRECISION = lax.Precision.HIGHEST


def recurrent(
    query_f, key_all, value_all, gate_in, gate_forget, accepted, memory, normalizer, stabilizer
):
    proposals = query_f.shape[1]
    total_span = key_all.shape[1]
    position = jnp.arange(total_span, dtype=jnp.int32)
    dropped = (position[None, :] < proposals) & (position[None, :] >= accepted[:, None])
    forget = jnp.where(dropped[:, :, None], 0.0, gate_forget)
    inflow = jnp.where(dropped[:, :, None], FAR_NEGATIVE, gate_in)
    running = jnp.cumsum(forget, axis=1)
    latest = running[:, proposals:]
    spread = latest[:, :, None, :] - running[:, None, :, :] + inflow[:, None, :, :]
    causal = position[None, :] <= (proposals + jnp.arange(proposals, dtype=jnp.int32))[:, None]
    spread = jnp.where(causal[None, :, :, None], spread, FAR_NEGATIVE)
    carried = latest + stabilizer[:, None, :]
    ceiling = jnp.maximum(jnp.max(spread, axis=2), carried)
    scores = jnp.einsum("sthk,suhk->stuh", query_f, key_all, precision=HIGHEST_PRECISION)
    weights = jnp.exp(spread - ceiling[:, :, None, :]) * scores
    carry_scale = jnp.exp(carried - ceiling)
    numerator = jnp.einsum("stuh,suhv->sthv", weights, value_all, precision=HIGHEST_PRECISION)
    numerator = numerator + carry_scale[..., None] * jnp.einsum(
        "shvk,sthk->sthv", memory, query_f, precision=HIGHEST_PRECISION
    )
    denominator = jnp.sum(weights, axis=2) + carry_scale * jnp.einsum(
        "shk,sthk->sth", normalizer, query_f, precision=HIGHEST_PRECISION
    )
    cell_out = numerator / jnp.maximum(jnp.abs(denominator), jnp.exp(-ceiling))[..., None]
    boundary = running[:, proposals - 1]
    reached = boundary[:, None, :] - running[:, :proposals] + inflow[:, :proposals]
    new_stabilizer = jnp.maximum(boundary + stabilizer, jnp.max(reached, axis=1))
    decay_old = jnp.exp(boundary + stabilizer - new_stabilizer)
    shares = jnp.exp(reached - new_stabilizer[:, None, :])
    new_memory = decay_old[:, :, None, None] * memory + jnp.einsum(
        "sjh,sjhv,sjhk->shvk",
        shares,
        value_all[:, :proposals],
        key_all[:, :proposals],
        precision=HIGHEST_PRECISION,
    )
    new_normalizer = decay_old[:, :, None] * normalizer + jnp.einsum(
        "sjh,sjhk->shk", shares, key_all[:, :proposals], precision=HIGHEST_PRECISION
    )
    return (cell_out, new_memory, new_normalizer, new_stabilizer)


def shards(
    tokens,
    norm_gain,
    w_query,
    w_key,
    w_value,
    w_outgate,
    w_input,
    w_forget,
    forget_bias,
    head_gain,
    w_out,
    memory,
    normalizer,
    stabilizer,
    prev_keys,
    prev_values,
    prev_input,
    prev_forget,
    accepted,
):
    sequences, proposals, columns = tokens.shape
    model_width = w_query.shape[0]
    local_heads = w_query.shape[1]
    key_size = w_query.shape[2]
    value_part = w_value.shape[2]
    token_rows = sequences * proposals
    head_start = lax.axis_index("kv") * local_heads
    value_start = lax.axis_index("tp") * value_part
    input_cols = lax.dynamic_slice_in_dim(w_input, head_start, local_heads, 1)
    forget_cols = lax.dynamic_slice_in_dim(w_forget, head_start, local_heads, 1)
    forget_shift = lax.dynamic_slice_in_dim(forget_bias, head_start, local_heads, 0)
    gain_block = lax.dynamic_slice(head_gain, (head_start, value_start), (local_heads, value_part))
    gathered = lax.all_gather(tokens, ("kv", "tp"), axis=2, tiled=True)
    as_float = gathered.astype(jnp.float32)
    inv_scale = lax.rsqrt(jnp.mean(as_float * as_float, axis=-1, keepdims=True) + EPS)
    normed = (as_float * inv_scale * norm_gain).astype(jnp.bfloat16)
    normed = normed.reshape(token_rows, model_width)

    def project(weight):
        return jnp.dot(normed, weight.reshape(model_width, -1), preferred_element_type=jnp.float32)

    queries = (
        project(w_query).astype(jnp.bfloat16).reshape(sequences, proposals, local_heads, key_size)
    )
    new_keys = (
        project(w_key).astype(jnp.bfloat16).reshape(sequences, proposals, local_heads, key_size)
    )
    new_values = (
        project(w_value).astype(jnp.bfloat16).reshape(sequences, proposals, local_heads, value_part)
    )
    out_gate = project(w_outgate).reshape(sequences, proposals, local_heads, value_part)
    new_input = project(input_cols).reshape(sequences, proposals, local_heads)
    new_forget = jax.nn.log_sigmoid(
        project(forget_cols).reshape(sequences, proposals, local_heads) + forget_shift
    )
    query_f = queries.astype(jnp.float32) * key_size ** (-0.5)
    key_all = jnp.concatenate([prev_keys, new_keys], axis=1).astype(jnp.float32)
    value_all = jnp.concatenate([prev_values, new_values], axis=1).astype(jnp.float32)
    gate_in = jnp.concatenate([prev_input, new_input], axis=1)
    gate_forget = jnp.concatenate([prev_forget, new_forget], axis=1)
    cell_out, new_memory, new_normalizer, new_stabilizer = recurrent(
        query_f, key_all, value_all, gate_in, gate_forget, accepted, memory, normalizer, stabilizer
    )
    head_squares = lax.psum(jnp.sum(cell_out * cell_out, axis=-1), "tp")
    full_values = value_part * lax.axis_size("tp")
    inv_head = lax.rsqrt(head_squares / full_values + EPS)
    gated = (jax.nn.sigmoid(out_gate) * cell_out * inv_head[..., None] * gain_block).astype(
        jnp.bfloat16
    )
    flat_rows = gated.reshape(token_rows, local_heads * value_part)
    out_block = lax.all_to_all(
        w_out.reshape(1, local_heads * value_part, model_width),
        ("kv", "tp"),
        split_axis=2,
        concat_axis=0,
        tiled=True,
    )
    summed = jnp.einsum(
        "gtc,gcd->td",
        lax.all_gather(
            flat_rows.reshape(1, token_rows, local_heads * value_part),
            ("kv", "tp"),
            axis=0,
            tiled=True,
        ),
        out_block,
        preferred_element_type=jnp.float32,
    )
    mixed = summed.astype(jnp.bfloat16).reshape(sequences, proposals, out_block.shape[2])
    return (
        mixed,
        new_memory,
        new_normalizer,
        new_stabilizer,
        new_keys,
        new_values,
        new_input,
        new_forget,
    )


def solution(mesh):
    return jax.shard_map(
        shards,
        mesh=mesh,
        in_specs=(
            P(("grp", "dp"), None, ("kv", "tp")),
            P(),
            P(None, "kv", None),
            P(None, "kv", None),
            P(None, "kv", "tp"),
            P(None, "kv", "tp"),
            P(),
            P(),
            P(),
            P(),
            P("kv", "tp", None),
            P(("grp", "dp"), "kv", "tp", None),
            P(("grp", "dp"), "kv", None),
            P(("grp", "dp"), "kv"),
            P(("grp", "dp"), None, "kv", None),
            P(("grp", "dp"), None, "kv", "tp"),
            P(("grp", "dp"), None, "kv"),
            P(("grp", "dp"), None, "kv"),
            P(("grp", "dp")),
        ),
        out_specs=(
            P(("grp", "dp"), None, ("kv", "tp")),
            P(("grp", "dp"), "kv", "tp", None),
            P(("grp", "dp"), "kv", None),
            P(("grp", "dp"), "kv"),
            P(("grp", "dp"), None, "kv", None),
            P(("grp", "dp"), None, "kv", "tp"),
            P(("grp", "dp"), None, "kv"),
            P(("grp", "dp"), None, "kv"),
        ),
        check_vma=False,
    )
```

profile of v0, /device:TPU:0, one launch (start us, length us, event | category | flops | bytes accessed | tf_op | source)
XLA Modules:
  0.0 165.0 jit_solution(10992848654207811287)
XLA Ops:
  7.2 0.0 copy-start
  7.2 0.0 all-gather.3.cloned.1.call-start
  7.2 0.7 all-gather.3.cloned.1.call-update
  7.9 10.0 %copy.164 = bf16[1,256,4096]{1,0,2:T(2,128)(2,1)} copy(bf16[1,256,4096]{2,1,0:T(8,128)(2,1)} %bitcast.117) | data formatting | bytes 4194304 | tf_op jit(solution)/shard_map/reshape | solution.py:128
  17.9 0.5 broadcast.99
  18.4 22.9 %reduce = bf16[4096,256]{1,0:T(8,128)(2,1)} reduce(bf16[4096,1,256]{2,1,0:T(2,128)(2,1)} %bitcast.114, bf16[]{:T(256)} %broadcast.99), dimensions={1}, to_apply=%bitcast.96.reduce_sub_computation | reduce | bytes 4194306
  41.3 5.8 %reshape.176 = bf16[8,2,65536]{2,1,0:T(2,128)(2,1)} reshape(bf16[4096,256]{1,0:T(8,128)(2,1)} %reduce) | data formatting | bytes 4194304
  47.1 6.5 %all-to-all-start = ((bf16[8,2,65536]{2,1,0:T(2,128)(2,1)}), bf16[8,2,65536]{2,1,0:T(2,128)(2,1)}, u32[]{:S(2)}, u32[]{:S(2)}) async-start(bf16[8,2,65536]{2,1,0:T(2,128)(2,1)} %reshape.176), calls=%async_computation | async-start | bytes 4194304 | tf_op jit(solution)/shard_map/all_to_all | solution.py:127
  53.6 0.0 all-gather.5.cloned.1.call-start
  53.7 0.1 copy.156
  53.8 0.8 copy.147
  54.6 0.1 dynamic_slice.13
  54.7 1.3 dynamic_slice.15
  56.0 0.1 iota_compare_fusion.1
  56.1 0.1 fusion.100
  56.2 2.9 %fusion = f32[64,4]{1,0:T(8,128)S(1)} fusion(bf16[64,4,4096]{2,1,0:T(4,128)(2,1)} %all-gather.3.cloned.1.call-done), kind=kLoop, calls=%fused_computation.3 | loop fusion | flops 3145472 | bytes 2098176 | tf_op jit(solution)/shard_map/reduce_sum | solution.py:91
  59.1 1.9 %fusion.2 = bf16[64,4,4096]{2,1,0:T(4,128)(2,1)S(1)} fusion(bf16[64,4,4096]{2,1,0:T(4,128)(2,1)S(1)} %copy-done.1, f32[4096]{0:T(1024)S(1)} %copy-done.19, f32[64,4]{1,0:T(8,128)S(1)} %add_rsqrt_fusion), kind=kLoop, calls=%fused_computation.5 | loop fusion | flops 4194304 | bytes 4211712 | tf_op jit(solution)/shard_map/convert_element_type | solution.py:92
  61.1 1.3 copy-done.2
  62.4 3.2 %fusion.90 = f32[64,4,4]{0,2,1:T(4,128)S(1)} fusion(bf16[4096,16]{0,1:T(8,128)(2,1)} %param.26, s32[]{:T(128)S(6)} %select_n.29, bf16[64,4,4096]{2,1,0:T(4,128)(2,1)S(1)} %fusion.2, f32[4]{0:T(128)S(1)} %dynamic_slice.13), kind=kOutput, calls=%fused_computation.66 | convolution fusion | flops 8397824 | bytes 2134036 | tf_op jit(solution)/shard_map/dot_general | solution.py:96
  65.6 0.1 copy.151
  65.7 0.4 copy-done.29
  66.2 4.0 %reshape.159 = bf16[256,4096]{1,0:T(8,128)(2,1)} reshape(bf16[64,4,4096]{2,1,0:T(4,128)(2,1)} %copy-done.2) | data formatting | bytes 4194304 | tf_op jit(solution)/shard_map/reshape | solution.py:93
  70.2 0.1 copy.150
  70.3 3.9 %fusion.8 = f32[64,4,4]{0,2,1:T(4,128)S(1)} fusion(bf16[64,4,4096]{2,1,0:T(4,128)(2,1)} %copy-done.2, bf16[4096,16]{0,1:T(8,128)(2,1)} %param.25, s32[]{:T(128)S(6)} %select_n.29), kind=kOutput, calls=%fused_computation.11 | convolution fusion | flops 8388608 | bytes 2134020 | tf_op jit(solution)/shard_map/dot_general | solution.py:96
  74.2 0.6 copy-done.30
  74.8 0.1 copy.153
  75.0 0.8 fusion.77
  75.8 0.1 copy.154
  75.9 0.6 fusion.109
  76.5 0.8 copy.155
  77.3 2.3 %fusion.35 = f32[256,256]{1,0:T(8,128)S(1)} fusion(bf16[256,4096]{1,0:T(8,128)(2,1)} %reshape.159, bf16[4096,256]{0,1:T(8,128)(2,1)S(1)} %bitcast.113), kind=kOutput, calls=%fused_computation.24 | convolution fusion | flops 537067520 | bytes 4456448 | tf_op jit(solution)/shard_map/dot_general | solution.py:96
  79.6 0.2 mul.94
  79.8 3.6 %convolution_convert_fusion.1 = bf16[256,256]{1,0:T(8,128)(2,1)} fusion(bf16[256,4096]{1,0:T(8,128)(2,1)} %reshape.159, bf16[4096,256]{0,1:T(8,128)(2,1)} %bitcast.121), kind=kOutput, calls=%fused_computation.25 | convolution fusion | flops 536936448 | bytes 4325376 | tf_op jit(solution)/shard_map/dot_general | solution.py:96
  83.5 1.1 reshape.163
  84.6 0.1 copy.157
  84.7 3.7 %convolution_convert_fusion.2 = bf16[256,256]{1,0:T(8,128)(2,1)} fusion(bf16[256,4096]{1,0:T(8,128)(2,1)} %reshape.159, bf16[4096,256]{0,1:T(8,128)(2,1)} %bitcast.122), kind=kOutput, calls=%fused_computation.26 | convolution fusion | flops 536936448 | bytes 4325376 | tf_op jit(solution)/shard_map/dot_general | solution.py:96
  88.4 3.1 %fusion.111 = (f32[64,4,4]{1,2,0:T(4,128)}, f32[64,4,8,4]{2,1,3,0:T(4,128)}) fusion(f32[64,4,4,64]{3,2,1,0:T(4,128)S(1)} %mul.94, bf16[64,4,4,64]{3,1,2,0:T(4,128)(2,1)S(1)} %copy.157, bf16[64,4,4,64]{3,1,2,0:T(4,128)(2,1)S(1)} %copy.156, f32[64,4,4]{1,2,0:T(4,128)S(1)} %copy-done.16, f32[64,8,4]{1,2,0:T(4,128)S(1)} %copy.153, f32[64,8,4]{1,2,0:T(4,128)S(1)} %copy.151, ...), kind=kOutput, calls=%fused_computation.95 | convolution fusion | flops 6863872 | bytes 585760 | tf_op jit(solution)/shard_map/sthk,suhk->stuh/dot_general | solution.py:27
  91.5 1.8 %fusion.80 = f32[64,4,1,4]{3,2,1,0:T(1,128)S(1)} fusion(f32[64,4,64,1]{2,3,1,0:T(1,128)S(1)} %bitcast.118, f32[64,4,4,64]{3,2,1,0:T(4,128)S(1)} %mul.94), kind=kOutput, calls=%fused_computation.51 | convolution fusion | flops 786432 | bytes 331776 | tf_op jit(solution)/shard_map/shk,sthk->sth/dot_general | solution.py:34
  93.3 1.1 reshape.161
  94.4 0.8 copy.148
  95.2 1.0 copy.162
  96.2 0.1 copy.173
  96.4 2.4 %fusion.67 = f32[64,4,64,4]{2,3,1,0:T(4,128)S(1)} fusion(f32[64,4,8,4]{2,1,3,0:T(4,128)} %get-tuple-element.16, bf16[64,4,4,64]{3,1,2,0:T(4,128)(2,1)} %copy.148, bf16[64,4,4,64]{3,1,2,0:T(4,128)(2,1)} %copy.147), kind=kOutput, calls=%fused_computation.34 | convolution fusion | flops 6815744 | bytes 557056 | tf_op jit(solution)/shard_map/stuh,suhv->sthv/dot_general | solution.py:30
  98.9 15.6 %fusion.78 = f32[64,4,4,64]{3,2,1,0:T(4,128)S(1)} fusion(f32[64,4,64,64]{3,2,1,0:T(8,128)} %param.30, f32[64,4,4,64]{3,2,1,0:T(4,128)S(1)} %mul.94), kind=kOutput, calls=%fused_computation.49 | convolution fusion | flops 50331648 | bytes 4718592 | tf_op jit(solution)/shard_map/shvk,sthk->sthv/dot_general | solution.py:31
  114.5 0.8 copy-done.3
  115.3 0.6 multiply_reduce_fusion
  115.9 2.6 %psum.7 = f32[64,4,4]{0,2,1:T(4,128)S(1)} all-reduce(f32[64,4,4]{0,2,1:T(4,128)S(1)} %multiply_reduce_fusion), channel_id=1, replica_groups=mesh['grp'=2,'dp'=2,'kv'=4,'tp'=2] {'tp'}, use_global_device_ids=true, to_apply=%region_5.6 | all-reduce | flops 1024 | bytes 8192 | tf_op jit(solution)/shard_map/psum | solution.py:120
  118.5 3.1 %fusion.126 = bf16[64,4,4096,1]{2,1,0,3:T(4,128)(2,1)S(1)} fusion(f32[4096]{0:T(1024)S(1)} %copy-done.20, f32[64,4]{1,0:T(8,128)S(1)} %copy-done.10, bf16[64,4,4096]{2,1,0:T(4,128)(2,1)} %all-gather.3.cloned.1.call-done), kind=kLoop, calls=%fused_computation.97 | loop fusion | flops 4194304 | bytes 4211712 | tf_op jit(solution)/shard_map/convert_element_type | solution.py:92
  121.7 2.1 %fusion.56 = bf16[64,4,4,64]{3,0,2,1:T(8,128)(2,1)S(1)} fusion(bf16[4096,4,64]{0,2,1:T(8,128)(2,1)S(1)} %copy-done.35, bf16[64,4,4096,1]{2,1,0,3:T(4,128)(2,1)S(1)} %fusion.126, f32[4,64]{1,0:T(4,128)S(1)} %copy-done.31, f32[64,4,4]{0,2,1:T(4,128)S(1)} %add_rsqrt_fusion.1, f32[64,4,4]{0,2,1:T(4,128)S(1)} %get-tuple-element.10, ...), kind=kOutput, calls=%fused_computation.31 | convolution fusion | flops 537526272 | bytes 4862976 | tf_op jit(solution)/shard_map/dot_general | solution.py:96
  123.9 0.2 copy.163
  124.1 0.9 reshape_reshape.3
  124.9 0.0 all-gather.5.cloned.1.call-update
  125.0 7.0 %reshape.177 = bf16[4096,1,256]{2,1,0:T(2,128)(2,1)} reshape(bf16[8,2,65536]{2,1,0:T(2,128)(2,1)} %all-to-all-done) | data formatting | bytes 4194304
  132.0 3.9 %copy.178 = bf16[1,256,4096]{1,2,0:T(8,128)(2,1)} copy(bf16[1,256,4096]{1,0,2:T(2,128)(2,1)} %bitcast.115) | data formatting | bytes 4194304
  135.9 4.0 %copy.165 = bf16[1,256,8,512]{3,1,2,0:T(8,128)(2,1)} copy(bf16[1,256,8,512]{1,3,2,0:T(8,128)(2,1)} %bitcast.116) | data formatting | bytes 4194304 | tf_op jit(solution)/shard_map/all_to_all | solution.py:127
  139.9 0.1 copy.167
  140.0 0.1 copy.166
  140.1 0.1 copy.174
  140.3 1.0 fusion.112
  141.3 0.8 multiply_add_fusion.1
  142.1 0.3 convert_multiply_fusion.2
  142.4 12.3 %multiply_add_fusion = f32[64,4,64,64]{3,2,1,0:T(8,128)} fusion(f32[64,4,64,64]{3,2,1,0:T(8,128)} %param.30, f32[64,4]{1,0:T(8,128)S(1)} %copy.166, bf16[64,4,4,64]{3,1,2,0:T(4,128)(2,1)S(1)} %copy.156, f32[64,4,4,64]{3,2,1,0:T(4,128)S(1)} %convert_multiply_fusion.2), kind=kOutput, calls=%fused_computation | convolution fusion | flops 52428800 | bytes 8782848 | tf_op jit(solution)/shard_map/sjh,sjhv,sjhk->shvk/dot_general | solution.py:43
  154.7 2.6 %fusion.31 = bf16[256,512]{1,0:T(8,128)(2,1)S(1)} fusion(bf16[8,256,256]{2,1,0:T(8,128)(2,1)} %all-gather.5.cloned.1.call-done, bf16[1,256,8,512]{3,1,2,0:T(8,128)(2,1)} %copy.165), kind=kOutput, calls=%fused_computation.21 | convolution fusion | flops 537001984 | bytes 3407872 | tf_op jit(solution)/shard_map/gtc,gcd->td/dot_general | solution.py:134
  157.3 0.8 reshape.166
  (82 shorter events, 0.3 us)
Async XLA Ops:
  7.2 70.1 %copy-start = (bf16[4096,4,64]{0,2,1:T(8,128)(2,1)S(1)}, bf16[4096,4,64]{0,2,1:T(8,128)(2,1)}, u32[]{:S(2)}) copy-start(bf16[4096,4,64]{0,2,1:T(8,128)(2,1)} %param.21) | copy-start | bytes 6291460
  7.2 49.0 %all-gather.3.cloned.1.call-start = ((), (), s32[]{:S(2)}) async-start(), calls=%async_computation.1 | async-start | bytes 2359296 | tf_op jit(solution)/shard_map/all_gather | solution.py:89
  47.1 6.6 %copy-start.11 = (bf16[64,4,4,64]{3,2,1,0:T(4,128)(2,1)S(1)}, bf16[64,4,4,64]{3,2,1,0:T(4,128)(2,1)}, u32[]{:S(2)}) copy-start(bf16[64,4,4,64]{3,2,1,0:T(4,128)(2,1)} %param.33) | copy-start | bytes 393220
  47.1 6.7 %copy-start.5 = (bf16[64,4,4,64]{3,2,1,0:T(4,128)(2,1)S(1)}, bf16[64,4,4,64]{3,2,1,0:T(4,128)(2,1)}, u32[]{:S(2)}) copy-start(bf16[64,4,4,64]{3,2,1,0:T(4,128)(2,1)} %param.34) | copy-start | bytes 393220
  47.1 7.5 %copy-start.36 = (f32[16]{0:T(128)S(1)}, f32[16]{0:T(128)}, u32[]{:S(2)}) copy-start(f32[16]{0:T(128)} %param.27) | copy-start | bytes 196
  47.1 9.0 %copy-start.34 = (s32[64]{0:T(128)S(1)}, s32[64]{0:T(128)}, u32[]{:S(2)}) copy-start(s32[64]{0:T(128)} %param.37) | copy-start | bytes 772
  47.1 77.9 %all-to-all-start = ((bf16[8,2,65536]{2,1,0:T(2,128)(2,1)}), bf16[8,2,65536]{2,1,0:T(2,128)(2,1)}, u32[]{:S(2)}, u32[]{:S(2)}) async-start(bf16[8,2,65536]{2,1,0:T(2,128)(2,1)} %reshape.176), calls=%async_computation | async-start | bytes 4194304 | tf_op jit(solution)/shard_map/all_to_all | solution.py:127
  53.6 5.5 %copy-start.19 = (f32[4096]{0:T(1024)S(1)}, f32[4096]{0:T(1024)}, u32[]{:S(2)}) copy-start(f32[4096]{0:T(1024)} %param.20) | copy-start | bytes 49156
  53.6 101.1 %all-gather.5.cloned.1.call-start = ((), (), s32[]{:S(2)}) async-start(), calls=%async_computation.2 | async-start | bytes 1179648 | tf_op jit(solution)/shard_map/all_gather | solution.py:136
  56.1 18.9 %copy-start.32 = (pred[4,8]{1,0:T(4,128)(4,1)}, pred[4,8]{1,0:T(4,128)(4,1)S(1)}, u32[]{:S(2)}) copy-start(pred[4,8]{1,0:T(4,128)(4,1)S(1)} %iota_compare_fusion.1) | copy-start | bytes 100
  56.2 2.9 %copy-start.1 = (bf16[64,4,4096]{2,1,0:T(4,128)(2,1)S(1)}, bf16[64,4,4096]{2,1,0:T(4,128)(2,1)}, u32[]{:S(2)}) copy-start(bf16[64,4,4096]{2,1,0:T(4,128)(2,1)} %all-gather.3.cloned.1.call-done) | copy-start | bytes 6291460
  59.1 1.9 %copy-start.9 = (f32[64,4]{1,0:T(8,128)}, f32[64,4]{1,0:T(8,128)S(1)}, u32[]{:S(2)}) copy-start(f32[64,4]{1,0:T(8,128)S(1)} %add_rsqrt_fusion) | copy-start | bytes 3076
  61.1 1.3 copy-start.2
  62.4 3.2 %copy-start.27 = (f32[64,4,4]{0,2,1:T(4,128)S(1)}, f32[64,4,4]{0,2,1:T(4,128)}, u32[]{:S(2)}) copy-start(f32[64,4,4]{0,2,1:T(4,128)} %param.36) | copy-start | bytes 12292
  65.6 0.6 copy-start.29
  66.2 9.7 %copy-start.23 = (f32[64,4]{0,1:T(4,128)}, f32[64,4]{0,1:T(4,128)S(1)}, u32[]{:S(2)}) copy-start(f32[64,4]{0,1:T(4,128)S(1)} %slice_bitcast_fusion) | copy-start | bytes 3076
  70.2 4.6 %copy-start.28 = (f32[64,4,4]{0,2,1:T(4,128)S(1)}, f32[64,4,4]{0,2,1:T(4,128)}, u32[]{:S(2)}) copy-start(f32[64,4,4]{0,2,1:T(4,128)} %param.35) | copy-start | bytes 12292
  70.2 5.7 %copy-start.21 = (f32[64,4]{0,1:T(4,128)S(1)}, f32[64,4]{0,1:T(4,128)}, u32[]{:S(2)}) copy-start(f32[64,4]{0,1:T(4,128)} %param.32) | copy-start | bytes 3076
  74.2 0.6 copy-start.30
  74.8 2.4 %copy-start.12 = (f32[64,8,4]{0,2,1:T(4,128)}, f32[64,8,4]{0,2,1:T(4,128)S(1)}, u32[]{:S(2)}) copy-start(f32[64,8,4]{0,2,1:T(4,128)S(1)} %maximum_select_fusion.2) | copy-start | bytes 24580
  76.5 0.8 copy-start.17
  84.5 3.8 %copy-start.7 = (bf16[64,4,4,64]{3,2,1,0:T(4,128)(2,1)}, bf16[64,4,4,64]{3,2,1,0:T(4,128)(2,1)S(1)}, u32[]{:S(2)}) copy-start(bf16[64,4,4,64]{3,2,1,0:T(4,128)(2,1)S(1)} %reshape.163) | copy-start | bytes 393220
  84.7 3.7 %copy-start.16 = (f32[64,4,4]{1,2,0:T(4,128)S(1)}, f32[64,4,4]{1,2,0:T(4,128)}, u32[]{:S(2)}) copy-start(f32[64,4,4]{1,2,0:T(4,128)} %copy.155) | copy-start | bytes 12292
  84.7 3.7 %copy-start.33 = (pred[4,8]{1,0:T(4,128)(4,1)S(1)}, pred[4,8]{1,0:T(4,128)(4,1)}, u32[]{:S(2)}) copy-start(pred[4,8]{1,0:T(4,128)(4,1)} %copy-done.32) | copy-start | bytes 100
  88.3 3.1 %copy-start.14 = (f32[64,4,64]{2,1,0:T(4,128)S(1)}, f32[64,4,64]{2,1,0:T(4,128)}, u32[]{:S(2)}) copy-start(f32[64,4,64]{2,1,0:T(4,128)} %param.31) | copy-start | bytes 196612
  91.4 4.9 %copy-start.22 = (f32[64,4]{0,1:T(4,128)S(1)}, f32[64,4]{0,1:T(4,128)}, u32[]{:S(2)}) copy-start(f32[64,4]{0,1:T(4,128)} %param.32) | copy-start | bytes 3076
  91.4 4.9 %copy-start.26 = (f32[64,4]{0,1:T(4,128)S(1)}, f32[64,4]{0,1:T(4,128)}, u32[]{:S(2)}) copy-start(f32[64,4]{0,1:T(4,128)} %get-tuple-element.13) | copy-start | bytes 3076
  91.4 4.9 %copy-start.13 = (f32[64,8,4]{0,2,1:T(4,128)S(1)}, f32[64,8,4]{0,2,1:T(4,128)}, u32[]{:S(2)}) copy-start(f32[64,8,4]{0,2,1:T(4,128)} %copy-done.12) | copy-start | bytes 24580
  91.4 4.9 %copy-start.18 = (f32[64,4,4]{0,2,1:T(4,128)S(1)}, f32[64,4,4]{0,2,1:T(4,128)}, u32[]{:S(2)}) copy-start(f32[64,4,4]{0,2,1:T(4,128)} %copy-done.17) | copy-start | bytes 12292
  91.4 4.9 %copy-start.24 = (f32[64,4]{0,1:T(4,128)S(1)}, f32[64,4]{0,1:T(4,128)}, u32[]{:S(2)}) copy-start(f32[64,4]{0,1:T(4,128)} %copy-done.23) | copy-start | bytes 3076
  94.4 2.0 %copy-start.8 = (bf16[64,4,4,64]{3,2,1,0:T(4,128)(2,1)}, bf16[64,4,4,64]{3,2,1,0:T(4,128)(2,1)S(1)}, u32[]{:S(2)}) copy-start(bf16[64,4,4,64]{3,2,1,0:T(4,128)(2,1)S(1)} %reshape.161) | copy-start | bytes 393220
  96.3 18.1 %copy-start.25 = (f32[64,4]{0,1:T(4,128)}, f32[64,4]{0,1:T(4,128)S(1)}, u32[]{:S(2)}) copy-start(f32[64,4]{0,1:T(4,128)S(1)} %get-tuple-element.9) | copy-start | bytes 3076
  98.8 19.7 %copy-start.10 = (f32[64,4]{1,0:T(8,128)S(1)}, f32[64,4]{1,0:T(8,128)}, u32[]{:S(2)}) copy-start(f32[64,4]{1,0:T(8,128)} %copy-done.9) | copy-start | bytes 3076
  98.9 19.7 %copy-start.20 = (f32[4096]{0:T(1024)S(1)}, f32[4096]{0:T(1024)}, u32[]{:S(2)}) copy-start(f32[4096]{0:T(1024)} %param.20) | copy-start | bytes 49156
  114.5 0.8 copy-start.3
  118.5 3.2 %copy-start.4 = (f32[64,4,4,64]{3,2,1,0:T(4,128)S(1)}, f32[64,4,4,64]{3,2,1,0:T(4,128)}, u32[]{:S(2)}) copy-start(f32[64,4,4,64]{3,2,1,0:T(4,128)} %copy-done.3) | copy-start | bytes 786436
  118.5 3.2 %copy-start.31 = (f32[4,64]{1,0:T(4,128)S(1)}, f32[4,64]{1,0:T(4,128)}, u32[]{:S(2)}) copy-start(f32[4,64]{1,0:T(4,128)} %dynamic_slice.15) | copy-start | bytes 3076
  118.5 3.2 %copy-start.35 = (bf16[4096,4,64]{0,2,1:T(8,128)(2,1)S(1)}, bf16[4096,4,64]{0,2,1:T(8,128)(2,1)}, u32[]{:S(2)}) copy-start(bf16[4096,4,64]{0,2,1:T(8,128)(2,1)} %param.24) | copy-start | bytes 6291460
  135.9 5.3 %copy-start.15 = (f32[64,4,64]{2,1,0:T(4,128)S(1)}, f32[64,4,64]{2,1,0:T(4,128)}, u32[]{:S(2)}) copy-start(f32[64,4,64]{2,1,0:T(4,128)} %param.31) | copy-start | bytes 196612
  135.9 6.1 %copy-start.6 = (bf16[64,4,4,64]{3,2,1,0:T(4,128)(2,1)S(1)}, bf16[64,4,4,64]{3,2,1,0:T(4,128)(2,1)}, u32[]{:S(2)}) copy-start(bf16[64,4,4,64]{3,2,1,0:T(4,128)(2,1)} %param.34) | copy-start | bytes 393220
Sparse Core Ops, SparseCore 0:
  9.6 33.3 all-gather.2
  125.1 23.5 all-gather.4
where the time goes:
time: 166 us; the launch traced here: 165 us
  matrix products  57.6 us (35%)
  local copies, waits for them, and re-layouts  48.6 us (29%)
  other arithmetic  34.2 us (21%)
  between operations  14.6 us (9%)
  starting transfers between devices  6.58 us (4%)
  blocking collectives  2.62 us (2%)
    unnamed x1, other arithmetic  22.9 us
    unnamed x80, local copies, waits for them, and re-layouts  21.5 us
    dot_general x6, matrix products, project(): jnp.dot(normed, weight.reshape(model_width, -1), preferred_element_type=j...  18.8 us
    dot_general x1, matrix products, recurrent(): jnp.einsum('shvk,sthk->sthv', memory, query_f, precision=HIGHEST_PRECISION)  15.6 us
    dot_general x1, matrix products, recurrent(): jnp.einsum('sjh,sjhv,sjhk->shvk', shares, value_all[:, :proposals], key_a...  12.3 us
    reshape x1, local copies, waits for them, and re-layouts, shards(): w_out.reshape(1, local_heads * value_part, model_width)  9.96 us
    all_to_all x1, starting transfers between devices, shards(): lax.all_to_all(w_out.reshape(1, local_heads * value_part, model_width), (...  6.5 us
    convert_element_type x2, other arithmetic, shards(): normed = (as_float * inv_scale * norm_gain).astype(jnp.bfloat16)  5.06 us
  transfers between devices with their start and end apart: 3, of which 0 were waited for; matrix products, arithmetic and copies ran while one was open for 81% of the time, Pallas kernels for 0%

commit v1 on v0

--- a/solution.py
+++ b/solution.py
@@ -124,12 +124,20 @@
         jnp.bfloat16
     )
     flat_rows = gated.reshape(token_rows, local_heads * value_part)
-    out_block = lax.all_to_all(
-        w_out.reshape(1, local_heads * value_part, model_width),
-        ("kv", "tp"),
-        split_axis=2,
-        concat_axis=0,
-        tiled=True,
+    out_block = jnp.concatenate(
+        lax.all_to_all(
+            jnp.stack(
+                jnp.split(
+                    w_out.reshape(1, local_heads * value_part, model_width),
+                    lax.axis_size(("kv", "tp")),
+                    axis=2,
+                )
+            ),
+            ("kv", "tp"),
+            0,
+            0,
+        ),
+        axis=0,
     )
     summed = jnp.einsum(
         "gtc,gcd->td",

time: 166 us -> 160 us (0.964)
  waiting for transfers between devices: 0.7 us -> 40.1 us
  local copies, waits for them, and re-layouts: 48.6 us -> 26.9 us
  other arithmetic: 34.2 us -> 12.6 us
    all_gather x1, waiting for transfers between devices: 0.01 us -> 31.9 us  [shards(): gathered = lax.all_gather(tokens, ('kv', 'tp'), axis=2, tiled=True)]
    unnamed x1 -> x0, other arithmetic: 22.9 us -> none
    reshape x1 -> x0, local copies, waits for them, and re-layouts: 9.96 us -> none  [shards(): w_out.reshape(1, local_heads * value_part, model_width)]
    unnamed x80 -> x91, local copies, waits for them, and re-layouts: 21.5 us -> 12.7 us
    all_gather x1, waiting for transfers between devices: 0.01 us -> 7.44 us  [shards(): lax.all_gather(flat_rows.reshape(1, token_rows, local_heads * value_part)...]
    all_to_all x1 -> x0, local copies, waits for them, and re-layouts: 3.98 us -> none  [shards(): lax.all_to_all(w_out.reshape(1, local_heads * value_part, model_width), (...]
  transfers between devices with their start and end apart: 3 -> 3, of which waited for: 0 -> 2; matrix products, arithmetic and copies ran while one was open for 81% -> 56% of each run, Pallas kernels for 0% -> 0%
where the time goes in v1:
time: 160 us
  matrix products  56.2 us (35%)
  waiting for transfers between devices  40.1 us (25%)
  local copies, waits for them, and re-layouts  26.9 us (17%)
  between operations  14.7 us (9%)
  other arithmetic  12.6 us (8%)
  starting transfers between devices  6.58 us (4%)
  blocking collectives  2.5 us (2%)
    all_gather x1, waiting for transfers between devices, shards(): gathered = lax.all_gather(tokens, ('kv', 'tp'), axis=2, tiled=True)  31.9 us
    dot_general x6, matrix products, project(): jnp.dot(normed, weight.reshape(model_width, -1), preferred_element_type=j...  18.1 us
    dot_general x1, matrix products, recurrent(): jnp.einsum('shvk,sthk->sthv', memory, query_f, precision=HIGHEST_PRECISION)  15.7 us
    unnamed x91, local copies, waits for them, and re-layouts  12.7 us
    dot_general x1, matrix products, recurrent(): jnp.einsum('sjh,sjhv,sjhk->shvk', shares, value_all[:, :proposals], key_a...  12.3 us
    all_gather x1, waiting for transfers between devices, shards(): lax.all_gather(flat_rows.reshape(1, token_rows, local_heads * value_part)...  7.44 us
    all_to_all x1, starting transfers between devices, shards(): lax.all_to_all(jnp.stack(jnp.split(w_out.reshape(1, local_heads * value_p...  6.5 us
    convert_element_type x2, other arithmetic, shards(): normed = (as_float * inv_scale * norm_gain).astype(jnp.bfloat16)  5.06 us
  transfers between devices with their start and end apart: 3, of which 2 were waited for; matrix products, arithmetic and copies ran while one was open for 56% of the time, Pallas kernels for 0%

profile of v1, /device:TPU:0, one launch (start us, length us, event | category | flops | bytes accessed | tf_op | source)
XLA Modules:
  0.0 159.5 jit_solution(5907777759631301396)
XLA Ops:
  7.2 0.7 all-gather.3.cloned.1.call-update
  7.9 1.8 %fusion.90 = bf16[8,1,256,512]{3,2,1,0:T(8,128)(2,1)} fusion(bf16[1,256,4096]{2,1,0:T(8,128)(2,1)} %bitcast.141), kind=kLoop, calls=%fused_computation.69 | loop fusion | bytes 524288
  9.8 1.7 %fusion.89 = bf16[8,1,256,512]{3,2,1,0:T(8,128)(2,1)} fusion(bf16[8,1,256,512]{3,2,1,0:T(8,128)(2,1)} %fusion.90, bf16[1,256,4096]{2,1,0:T(8,128)(2,1)} %bitcast.142), kind=kLoop, calls=%fused_computation.67 | loop fusion | bytes 524288
  11.5 1.7 %fusion.88 = bf16[8,1,256,512]{3,2,1,0:T(8,128)(2,1)} fusion(bf16[8,1,256,512]{3,2,1,0:T(8,128)(2,1)} %fusion.89, bf16[1,256,4096]{2,1,0:T(8,128)(2,1)} %bitcast.143), kind=kLoop, calls=%fused_computation.65 | loop fusion | bytes 524288
  13.1 1.6 %fusion.87 = bf16[8,1,256,512]{3,2,1,0:T(8,128)(2,1)} fusion(bf16[8,1,256,512]{3,2,1,0:T(8,128)(2,1)} %fusion.88, bf16[1,256,4096]{2,1,0:T(8,128)(2,1)} %bitcast.144), kind=kLoop, calls=%fused_computation.63 | loop fusion | bytes 524288
  14.8 0.7 fusion.86
  15.5 0.7 fusion.85
  16.2 0.8 fusion.84
  17.0 0.7 fusion.83
  17.7 6.5 %all-to-all-start = ((bf16[8,1,256,512]{3,2,1,0:T(8,128)(2,1)}), bf16[8,1,256,512]{3,2,1,0:T(8,128)(2,1)}, u32[]{:S(2)}, u32[]{:S(2)}) async-start(bf16[8,1,256,512]{3,2,1,0:T(8,128)(2,1)} %fusion.83), calls=%async_computation | async-start | bytes 4194304 | tf_op jit(solution)/shard_map/all_to_all | solution.py:128
  24.2 0.0 all-gather.5.cloned.1.call-start
  24.3 0.1 copy.141
  24.4 0.8 copy.132
  25.3 0.1 dynamic_slice.13
  25.3 1.3 dynamic_slice.15
  26.7 0.1 iota_compare_fusion.1
  26.8 0.1 fusion.108
  26.8 31.9 %all-gather.3.cloned.1.call-done = bf16[64,4,4096]{2,1,0:T(4,128)(2,1)} async-done(((bf16[64,4,512]{2,1,0:T(4,128)(2,1)}), bf16[64,4,4096]{2,1,0:T(4,128)(2,1)}) %all-gather.3.cloned.1.call-update) | async-done | bytes 2097168 | tf_op jit(solution)/shard_map/all_gather | solution.py:89
  58.8 2.9 %fusion = f32[64,4]{1,0:T(8,128)S(1)} fusion(bf16[64,4,4096]{2,1,0:T(4,128)(2,1)} %all-gather.3.cloned.1.call-done), kind=kLoop, calls=%fused_computation.3 | loop fusion | flops 3145472 | bytes 2098176 | tf_op jit(solution)/shard_map/reduce_sum | solution.py:91
  61.7 1.9 %fusion.2 = bf16[64,4,4096]{2,1,0:T(4,128)(2,1)S(1)} fusion(bf16[64,4,4096]{2,1,0:T(4,128)(2,1)S(1)} %copy-done.1, f32[4096]{0:T(1024)S(1)} %copy-done.22, f32[64,4]{1,0:T(8,128)S(1)} %add_rsqrt_fusion), kind=kLoop, calls=%fused_computation.5 | loop fusion | flops 4194304 | bytes 4211712 | tf_op jit(solution)/shard_map/convert_element_type | solution.py:92
  63.7 1.3 copy-done.2
  65.0 3.2 %fusion.98 = f32[64,4,4]{0,2,1:T(4,128)S(1)} fusion(bf16[4096,16]{0,1:T(8,128)(2,1)} %param.26, s32[]{:T(128)S(6)} %select_n.29, bf16[64,4,4096]{2,1,0:T(4,128)(2,1)S(1)} %fusion.2, f32[4]{0:T(128)S(1)} %dynamic_slice.13), kind=kOutput, calls=%fused_computation.82 | convolution fusion | flops 8397824 | bytes 2134036 | tf_op jit(solution)/shard_map/dot_general | solution.py:96
  68.2 0.6 copy-done.34
  68.8 0.1 copy.136
  68.9 4.2 %reshape.162 = bf16[256,4096]{1,0:T(8,128)(2,1)} reshape(bf16[64,4,4096]{2,1,0:T(4,128)(2,1)} %copy-done.2) | data formatting | bytes 4194304 | tf_op jit(solution)/shard_map/reshape | solution.py:93
  73.1 0.1 copy.135
  73.2 3.9 %fusion.8 = f32[64,4,4]{0,2,1:T(4,128)S(1)} fusion(bf16[64,4,4096]{2,1,0:T(4,128)(2,1)} %copy-done.2, bf16[4096,16]{0,1:T(8,128)(2,1)} %param.25, s32[]{:T(128)S(6)} %select_n.29), kind=kOutput, calls=%fused_computation.11 | convolution fusion | flops 8388608 | bytes 2134020 | tf_op jit(solution)/shard_map/dot_general | solution.py:96
  77.2 0.6 copy-done.35
  77.8 0.1 copy.138
  77.9 0.8 fusion.77
  78.7 0.1 copy.139
  78.8 0.6 fusion.117
  79.4 0.8 copy.140
  80.2 2.3 %fusion.35 = f32[256,256]{1,0:T(8,128)S(1)} fusion(bf16[256,4096]{1,0:T(8,128)(2,1)} %reshape.162, bf16[4096,256]{0,1:T(8,128)(2,1)S(1)} %bitcast.140), kind=kOutput, calls=%fused_computation.24 | convolution fusion | flops 537067520 | bytes 4456448 | tf_op jit(solution)/shard_map/dot_general | solution.py:96
  82.6 0.2 mul.94
  82.8 3.0 %convolution_convert_fusion.1 = bf16[256,256]{1,0:T(8,128)(2,1)S(1)} fusion(bf16[256,4096]{1,0:T(8,128)(2,1)} %reshape.162, bf16[4096,256]{0,1:T(8,128)(2,1)} %bitcast.152), kind=kOutput, calls=%fused_computation.25 | convolution fusion | flops 536936448 | bytes 4325376 | tf_op jit(solution)/shard_map/dot_general | solution.py:96
  85.8 0.2 reshape.166
  86.0 0.8 copy.142
  86.8 3.6 %convolution_convert_fusion.2 = bf16[256,256]{1,0:T(8,128)(2,1)} fusion(bf16[256,4096]{1,0:T(8,128)(2,1)} %reshape.162, bf16[4096,256]{0,1:T(8,128)(2,1)} %bitcast.153), kind=kOutput, calls=%fused_computation.26 | convolution fusion | flops 536936448 | bytes 4325376 | tf_op jit(solution)/shard_map/dot_general | solution.py:96
  90.4 1.1 reshape.164
  91.5 0.8 copy.133
  92.3 1.3 subtract_exponential_fusion.2
  93.6 3.5 %fusion.119 = (f32[64,4,4]{1,2,0:T(4,128)S(1)}, f32[64,4,8,4]{2,1,3,0:T(4,128)}) fusion(f32[64,4,4,64]{3,2,1,0:T(4,128)S(1)} %mul.94, bf16[64,4,4,64]{3,1,2,0:T(4,128)(2,1)} %copy.142, bf16[64,4,4,64]{3,1,2,0:T(4,128)(2,1)S(1)} %copy.141, f32[64,4,4]{1,2,0:T(4,128)} %copy.140, f32[64,8,4]{1,2,0:T(4,128)} %copy-done.12, f32[64,8,4]{1,2,0:T(4,128)S(1)} %copy.136, ...), kind=kOutput, calls=%fused_computation.111 | convolution fusion | flops 6863872 | bytes 585760 | tf_op jit(solution)/shard_map/sthk,suhk->stuh/dot_general | solution.py:27
  97.1 0.7 copy.147
  97.8 1.8 %fusion.80 = f32[64,4,1,4]{3,2,1,0:T(1,128)S(1)} fusion(f32[64,4,64,1]{2,3,1,0:T(1,128)S(1)} %bitcast.149, f32[64,4,4,64]{3,2,1,0:T(4,128)S(1)} %mul.94), kind=kOutput, calls=%fused_computation.51 | convolution fusion | flops 786432 | bytes 331776 | tf_op jit(solution)/shard_map/shk,sthk->sth/dot_general | solution.py:34
  99.6 0.7 copy.156
  100.4 15.7 %fusion.78 = f32[64,4,4,64]{3,2,1,0:T(4,128)S(1)} fusion(f32[64,4,64,64]{3,2,1,0:T(8,128)} %param.30, f32[64,4,4,64]{3,2,1,0:T(4,128)S(1)} %mul.94), kind=kOutput, calls=%fused_computation.49 | convolution fusion | flops 50331648 | bytes 4718592 | tf_op jit(solution)/shard_map/shvk,sthk->sthv/dot_general | solution.py:31
  116.2 1.2 fusion.67
  117.5 0.6 multiply_reduce_fusion
  118.1 2.5 %psum.7 = f32[64,4,4]{0,2,1:T(4,128)S(1)} all-reduce(f32[64,4,4]{0,2,1:T(4,128)S(1)} %multiply_reduce_fusion), channel_id=1, replica_groups=mesh['grp'=2,'dp'=2,'kv'=4,'tp'=2] {'tp'}, use_global_device_ids=true, to_apply=%region_5.6 | all-reduce | flops 1024 | bytes 8192 | tf_op jit(solution)/shard_map/psum | solution.py:120
  120.6 3.1 %fusion.134 = bf16[64,4,4096,1]{2,1,0,3:T(4,128)(2,1)S(1)} fusion(f32[4096]{0:T(1024)S(1)} %copy-done.23, f32[64,4]{1,0:T(8,128)S(1)} %copy-done.14, bf16[64,4,4096]{2,1,0:T(4,128)(2,1)} %all-gather.3.cloned.1.call-done), kind=kLoop, calls=%fused_computation.113 | loop fusion | flops 4194304 | bytes 4211712 | tf_op jit(solution)/shard_map/convert_element_type | solution.py:92
  123.8 2.1 %fusion.56 = bf16[64,4,4,64]{3,0,2,1:T(8,128)(2,1)S(1)} fusion(bf16[4096,4,64]{0,2,1:T(8,128)(2,1)S(1)} %copy-done.39, bf16[64,4,4096,1]{2,1,0,3:T(4,128)(2,1)S(1)} %fusion.134, f32[4,64]{1,0:T(4,128)S(1)} %copy-done.36, f32[64,4,4]{0,2,1:T(4,128)S(1)} %add_rsqrt_fusion.1, f32[64,4,4]{0,2,1:T(4,128)S(1)} %get-tuple-element.10, ...), kind=kOutput, calls=%fused_computation.31 | convolution fusion | flops 537526272 | bytes 4862976 | tf_op jit(solution)/shard_map/dot_general | solution.py:96
  125.9 0.2 copy.148
  126.2 0.9 reshape_reshape.3
  127.1 0.1 copy.150
  127.2 0.1 copy.149
  127.3 0.1 copy.157
  127.4 1.0 fusion.120
  128.4 0.8 multiply_add_fusion.1
  129.2 0.3 convert_multiply_fusion.2
  129.5 12.3 %multiply_add_fusion = f32[64,4,64,64]{3,2,1,0:T(8,128)} fusion(f32[64,4,64,64]{3,2,1,0:T(8,128)} %param.30, f32[64,4]{1,0:T(8,128)S(1)} %copy.149, bf16[64,4,4,64]{3,1,2,0:T(4,128)(2,1)S(1)} %copy.141, f32[64,4,4,64]{3,2,1,0:T(4,128)S(1)} %convert_multiply_fusion.2), kind=kOutput, calls=%fused_computation | convolution fusion | flops 52428800 | bytes 8782848 | tf_op jit(solution)/shard_map/sjh,sjhv,sjhk->shvk/dot_general | solution.py:43
  141.8 7.4 %all-gather.5.cloned.1.call-done = bf16[8,256,256]{2,1,0:T(8,128)(2,1)} async-done(((bf16[1,256,256]{2,1,0:T(8,128)(2,1)}), bf16[8,256,256]{2,1,0:T(8,128)(2,1)}) %all-gather.5.cloned.1.call-update) | async-done | bytes 1048592 | tf_op jit(solution)/shard_map/all_gather | solution.py:144
  149.3 2.6 %fusion.31 = bf16[256,512]{1,0:T(8,128)(2,1)S(1)} fusion(bf16[8,256,256]{2,1,0:T(8,128)(2,1)} %all-gather.5.cloned.1.call-done, bf16[8,1,256,512]{3,2,1,0:T(8,128)(2,1)} %all-to-all-done), kind=kOutput, calls=%fused_computation.21 | convolution fusion | flops 537001984 | bytes 3407872 | tf_op jit(solution)/shard_map/gtc,gcd->td/dot_general | solution.py:142
  151.9 0.8 reshape.170
  (91 shorter events, 0.3 us)
Async XLA Ops:
  7.2 73.0 %copy-start = (bf16[4096,4,64]{0,2,1:T(8,128)(2,1)S(1)}, bf16[4096,4,64]{0,2,1:T(8,128)(2,1)}, u32[]{:S(2)}) copy-start(bf16[4096,4,64]{0,2,1:T(8,128)(2,1)} %param.21) | copy-start | bytes 6291460
  7.2 51.6 %all-gather.3.cloned.1.call-start = ((), (), s32[]{:S(2)}) async-start(), calls=%async_computation.1 | async-start | bytes 2359296 | tf_op jit(solution)/shard_map/all_gather | solution.py:89
  7.9 6.9 %copy-start.3 = (bf16[4,64,4096]{2,1,0:T(8,128)(2,1)S(1)}, bf16[4,64,4096]{2,1,0:T(8,128)(2,1)}, u32[]{:S(2)}) copy-start(bf16[4,64,4096]{2,1,0:T(8,128)(2,1)} %param.29) | copy-start | bytes 6291460
  17.7 6.6 %copy-start.15 = (bf16[64,4,4,64]{3,2,1,0:T(4,128)(2,1)S(1)}, bf16[64,4,4,64]{3,2,1,0:T(4,128)(2,1)}, u32[]{:S(2)}) copy-start(bf16[64,4,4,64]{3,2,1,0:T(4,128)(2,1)} %param.33) | copy-start | bytes 393220
  17.7 6.7 %copy-start.4 = (bf16[64,4,4,64]{3,2,1,0:T(4,128)(2,1)S(1)}, bf16[64,4,4,64]{3,2,1,0:T(4,128)(2,1)}, u32[]{:S(2)}) copy-start(bf16[64,4,4,64]{3,2,1,0:T(4,128)(2,1)} %param.34) | copy-start | bytes 393220
  17.7 7.5 %copy-start.40 = (f32[16]{0:T(128)S(1)}, f32[16]{0:T(128)}, u32[]{:S(2)}) copy-start(f32[16]{0:T(128)} %param.27) | copy-start | bytes 196
  17.7 9.0 %copy-start.38 = (s32[64]{0:T(128)S(1)}, s32[64]{0:T(128)}, u32[]{:S(2)}) copy-start(s32[64]{0:T(128)} %param.37) | copy-start | bytes 772
  17.7 124.1 %all-to-all-start = ((bf16[8,1,256,512]{3,2,1,0:T(8,128)(2,1)}), bf16[8,1,256,512]{3,2,1,0:T(8,128)(2,1)}, u32[]{:S(2)}, u32[]{:S(2)}) async-start(bf16[8,1,256,512]{3,2,1,0:T(8,128)(2,1)} %fusion.83), calls=%async_computation | async-start | bytes 4194304 | tf_op jit(solution)/shard_map/all_to_all | solution.py:128
  24.2 37.5 %copy-start.22 = (f32[4096]{0:T(1024)S(1)}, f32[4096]{0:T(1024)}, u32[]{:S(2)}) copy-start(f32[4096]{0:T(1024)} %param.20) | copy-start | bytes 49156
  24.2 125.0 %all-gather.5.cloned.1.call-start = ((), (), s32[]{:S(2)}) async-start(), calls=%async_computation.2 | async-start | bytes 1179648 | tf_op jit(solution)/shard_map/all_gather | solution.py:144
  26.8 51.2 %copy-start.37 = (pred[4,8]{1,0:T(4,128)(4,1)}, pred[4,8]{1,0:T(4,128)(4,1)S(1)}, u32[]{:S(2)}) copy-start(pred[4,8]{1,0:T(4,128)(4,1)S(1)} %iota_compare_fusion.1) | copy-start | bytes 100
  58.8 2.9 %copy-start.1 = (bf16[64,4,4096]{2,1,0:T(4,128)(2,1)S(1)}, bf16[64,4,4096]{2,1,0:T(4,128)(2,1)}, u32[]{:S(2)}) copy-start(bf16[64,4,4096]{2,1,0:T(4,128)(2,1)} %all-gather.3.cloned.1.call-done) | copy-start | bytes 6291460
  61.7 1.9 %copy-start.13 = (f32[64,4]{1,0:T(8,128)}, f32[64,4]{1,0:T(8,128)S(1)}, u32[]{:S(2)}) copy-start(f32[64,4]{1,0:T(8,128)S(1)} %add_rsqrt_fusion) | copy-start | bytes 3076
  63.7 1.3 copy-start.2
  65.0 3.2 %copy-start.32 = (f32[64,4,4]{0,2,1:T(4,128)S(1)}, f32[64,4,4]{0,2,1:T(4,128)}, u32[]{:S(2)}) copy-start(f32[64,4,4]{0,2,1:T(4,128)} %param.36) | copy-start | bytes 12292
  68.2 0.6 copy-start.34
  68.9 9.9 %copy-start.28 = (f32[64,4]{0,1:T(4,128)}, f32[64,4]{0,1:T(4,128)S(1)}, u32[]{:S(2)}) copy-start(f32[64,4]{0,1:T(4,128)S(1)} %slice_bitcast_fusion.8) | copy-start | bytes 3076
  73.1 4.7 %copy-start.33 = (f32[64,4,4]{0,2,1:T(4,128)S(1)}, f32[64,4,4]{0,2,1:T(4,128)}, u32[]{:S(2)}) copy-start(f32[64,4,4]{0,2,1:T(4,128)} %param.35) | copy-start | bytes 12292
  73.1 5.7 %copy-start.26 = (f32[64,4]{0,1:T(4,128)S(1)}, f32[64,4]{0,1:T(4,128)}, u32[]{:S(2)}) copy-start(f32[64,4]{0,1:T(4,128)} %param.32) | copy-start | bytes 3076
  73.2 7.0 %copy-start.11 = (f32[64,4,4]{1,2,0:T(4,128)}, f32[64,4,4]{1,2,0:T(4,128)S(1)}, u32[]{:S(2)}) copy-start(f32[64,4,4]{1,2,0:T(4,128)S(1)} %copy.135) | copy-start | bytes 12292
  77.2 0.6 copy-start.35
  77.8 2.4 %copy-start.16 = (f32[64,8,4]{0,2,1:T(4,128)}, f32[64,8,4]{0,2,1:T(4,128)S(1)}, u32[]{:S(2)}) copy-start(f32[64,8,4]{0,2,1:T(4,128)S(1)} %maximum_select_fusion.2) | copy-start | bytes 24580
  77.9 2.3 %copy-start.12 = (f32[64,8,4]{1,2,0:T(4,128)}, f32[64,8,4]{1,2,0:T(4,128)S(1)}, u32[]{:S(2)}) copy-start(f32[64,8,4]{1,2,0:T(4,128)S(1)} %copy.138) | copy-start | bytes 24580
  79.4 0.8 copy-start.20
  85.9 4.4 %copy-start.6 = (bf16[64,4,4,64]{3,2,1,0:T(4,128)(2,1)}, bf16[64,4,4,64]{3,2,1,0:T(4,128)(2,1)S(1)}, u32[]{:S(2)}) copy-start(bf16[64,4,4,64]{3,2,1,0:T(4,128)(2,1)S(1)} %reshape.166) | copy-start | bytes 393220
  91.5 5.6 %copy-start.7 = (bf16[64,4,4,64]{3,2,1,0:T(4,128)(2,1)}, bf16[64,4,4,64]{3,2,1,0:T(4,128)(2,1)S(1)}, u32[]{:S(2)}) copy-start(bf16[64,4,4,64]{3,2,1,0:T(4,128)(2,1)S(1)} %reshape.164) | copy-start | bytes 393220
  93.6 4.2 %copy-start.18 = (f32[64,4,64]{2,1,0:T(4,128)S(1)}, f32[64,4,64]{2,1,0:T(4,128)}, u32[]{:S(2)}) copy-start(f32[64,4,64]{2,1,0:T(4,128)} %param.31) | copy-start | bytes 196612
  100.3 15.8 %copy-start.8 = (bf16[64,4,4,64]{3,1,2,0:T(4,128)(2,1)S(1)}, bf16[64,4,4,64]{3,1,2,0:T(4,128)(2,1)}, u32[]{:S(2)}) copy-start(bf16[64,4,4,64]{3,1,2,0:T(4,128)(2,1)} %copy.132) | copy-start | bytes 393220
  100.3 15.8 %copy-start.9 = (bf16[64,4,4,64]{3,1,2,0:T(4,128)(2,1)S(1)}, bf16[64,4,4,64]{3,1,2,0:T(4,128)(2,1)}, u32[]{:S(2)}) copy-start(bf16[64,4,4,64]{3,1,2,0:T(4,128)(2,1)} %copy.133) | copy-start | bytes 393220
  100.3 15.8 %copy-start.10 = (f32[64,4,8,4]{2,1,3,0:T(4,128)S(1)}, f32[64,4,8,4]{2,1,3,0:T(4,128)}, u32[]{:S(2)}) copy-start(f32[64,4,8,4]{2,1,3,0:T(4,128)} %get-tuple-element.16) | copy-start | bytes 98308
  100.3 17.0 %copy-start.17 = (f32[64,8,4]{0,2,1:T(4,128)S(1)}, f32[64,8,4]{0,2,1:T(4,128)}, u32[]{:S(2)}) copy-start(f32[64,8,4]{0,2,1:T(4,128)} %copy-done.16) | copy-start | bytes 24580
  100.4 17.0 %copy-start.21 = (f32[64,4,4]{0,2,1:T(4,128)S(1)}, f32[64,4,4]{0,2,1:T(4,128)}, u32[]{:S(2)}) copy-start(f32[64,4,4]{0,2,1:T(4,128)} %copy-done.20) | copy-start | bytes 12292
  100.4 17.0 %copy-start.24 = (f32[64,4,4]{0,2,1:T(4,128)S(1)}, f32[64,4,4]{0,2,1:T(4,128)}, u32[]{:S(2)}) copy-start(f32[64,4,4]{0,2,1:T(4,128)} %copy.147) | copy-start | bytes 12292
  100.4 17.0 %copy-start.25 = (f32[64,4,1,4]{0,1,3,2:T(4,128)S(1)}, f32[64,4,1,4]{0,1,3,2:T(4,128)}, u32[]{:S(2)}) copy-start(f32[64,4,1,4]{0,1,3,2:T(4,128)} %copy.156) | copy-start | bytes 12292
  100.4 17.0 %copy-start.27 = (f32[64,4]{0,1:T(4,128)S(1)}, f32[64,4]{0,1:T(4,128)}, u32[]{:S(2)}) copy-start(f32[64,4]{0,1:T(4,128)} %param.32) | copy-start | bytes 3076
  100.4 17.0 %copy-start.29 = (f32[64,4]{0,1:T(4,128)S(1)}, f32[64,4]{0,1:T(4,128)}, u32[]{:S(2)}) copy-start(f32[64,4]{0,1:T(4,128)} %copy-done.28) | copy-start | bytes 3076
  100.4 17.0 %copy-start.30 = (f32[64,4]{0,1:T(4,128)S(1)}, f32[64,4]{0,1:T(4,128)}, u32[]{:S(2)}) copy-start(f32[64,4]{0,1:T(4,128)} %get-tuple-element.9) | copy-start | bytes 3076
  116.1 4.4 %copy-start.14 = (f32[64,4]{1,0:T(8,128)S(1)}, f32[64,4]{1,0:T(8,128)}, u32[]{:S(2)}) copy-start(f32[64,4]{1,0:T(8,128)} %copy-done.13) | copy-start | bytes 3076
  116.1 4.5 %copy-start.23 = (f32[4096]{0:T(1024)S(1)}, f32[4096]{0:T(1024)}, u32[]{:S(2)}) copy-start(f32[4096]{0:T(1024)} %param.20) | copy-start | bytes 49156
  120.6 3.2 %copy-start.36 = (f32[4,64]{1,0:T(4,128)S(1)}, f32[4,64]{1,0:T(4,128)}, u32[]{:S(2)}) copy-start(f32[4,64]{1,0:T(4,128)} %dynamic_slice.15) | copy-start | bytes 3076
  120.6 3.2 %copy-start.39 = (bf16[4096,4,64]{0,2,1:T(8,128)(2,1)S(1)}, bf16[4096,4,64]{0,2,1:T(8,128)(2,1)}, u32[]{:S(2)}) copy-start(bf16[4096,4,64]{0,2,1:T(8,128)(2,1)} %param.24) | copy-start | bytes 6291460
  123.8 3.4 %copy-start.31 = (f32[64,4]{0,1:T(4,128)S(1)}, f32[64,4]{0,1:T(4,128)}, u32[]{:S(2)}) copy-start(f32[64,4]{0,1:T(4,128)} %get-tuple-element.8) | copy-start | bytes 3076
  125.9 2.5 %copy-start.19 = (f32[64,4,64]{2,1,0:T(4,128)S(1)}, f32[64,4,64]{2,1,0:T(4,128)}, u32[]{:S(2)}) copy-start(f32[64,4,64]{2,1,0:T(4,128)} %param.31) | copy-start | bytes 196612
  125.9 3.3 %copy-start.5 = (bf16[64,4,4,64]{3,2,1,0:T(4,128)(2,1)S(1)}, bf16[64,4,4,64]{3,2,1,0:T(4,128)(2,1)}, u32[]{:S(2)}) copy-start(bf16[64,4,4,64]{3,2,1,0:T(4,128)(2,1)} %param.34) | copy-start | bytes 393220
Sparse Core Ops, SparseCore 0:
  9.6 49.1 all-gather.2
  127.2 22.0 all-gather.4
